TPU v7x, 32 devices: a whole 2x2x4 slice. The times are simulated.
32 devices in a mesh: row: 8 (over z, core), col: 4 (over y, x).
Axes of the slice: x: 2, y: 2, z: 4, core: 2. Of those that a mesh axis runs over, the one named last changes fastest.
Arguments:
- streams: bfloat16 [3, 1, 4096, 512], P(None, None, ('row', 'col')), may hold values from -6 to 6
- filter_taps: float32 [2, 4096, 512], P(None, ('row', 'col')), may hold values from -4 to 4
- short_taps: float32 [3, 3, 512], replicated, may hold values from -3 to 3
- skip_gain: float32 [512], replicated, may hold values from -3 to 3
- out_weight: bfloat16 [512, 4096], replicated, may hold values from -0.25 to 0.25
Outputs:
- projected: bfloat16 [1, 4096, 4096], P(None, ('row', 'col'))
All inputs are finite; a program needn't handle non-finite values.
Results may differ from a plain program's by a relative error of at most 0.0049.
Values may be sent and summed in bfloat16 or wider, within the bound.
A program may use at most 64 MiB of HBM per device.

v0:
```python
import math

import jax
import jax.numpy as jnp
from jax import lax
from jax.sharding import PartitionSpec as P

HIGHEST_PRECISION = lax.Precision.HIGHEST
EPSILON = 1e-06


def with_halo(cells, sides, width):
    for axis, dim in sides:
        count = lax.axis_size(axis)
        ends = count - 1
        head = lax.slice_in_dim(cells, 0, width, axis=dim)
        tail = lax.slice_in_dim(cells, cells.shape[dim] - width, cells.shape[dim], axis=dim)
        cells = jnp.concatenate(
            [
                lax.ppermute(tail, axis, [(i, (i + 1) % count) for i in range(ends)]),
                cells,
                lax.ppermute(head, axis, [((i + 1) % count, i) for i in range(ends)]),
            ],
            axis=dim,
        )
    return cells


def unit_circle(numerator, period):
    angles = 2.0 * math.pi / period * (numerator % period).astype(jnp.float32)
    return (jnp.cos(angles), jnp.sin(angles))


def complex_times(left_real, left_imag, right_real, right_imag):
    return (
        left_real * right_real - left_imag * right_imag,
        left_real * right_imag + left_imag * right_real,
    )


def complex_einsum(formula, matrix_real, matrix_imag, operand_real, operand_imag):

    def single(matrix, operand):
        return jnp.einsum(formula, matrix, operand, precision=HIGHEST_PRECISION)

    return (
        single(matrix_real, operand_real) - single(matrix_imag, operand_imag),
        single(matrix_real, operand_imag) + single(matrix_imag, operand_real),
    )


def sequence_offsets(column_count, positions):
    blocks = jnp.arange(column_count, dtype=jnp.int32)
    within = jnp.arange(positions, dtype=jnp.int32)
    return (blocks, within, positions * blocks[:, None] + within[None, :])


def forward_rows(real_part, imag_part, frequencies, length):
    column_count, positions = (real_part.shape[1], real_part.shape[4])
    blocks, within, offsets = sequence_offsets(column_count, positions)
    cos_table, sin_table = unit_circle(frequencies[:, None, None] * offsets[None], length)
    real_part, imag_part = complex_times(
        real_part, imag_part, cos_table[:, :, None, None, :], -sin_table[:, :, None, None, :]
    )
    cos_table, sin_table = unit_circle(blocks[:, None] * blocks[None, :], column_count)
    real_part, imag_part = complex_einsum(
        "mc,rcbhj->rmbhj", cos_table, -sin_table, real_part, imag_part
    )
    cos_table, sin_table = unit_circle(blocks[:, None] * within[None, :], column_count * positions)
    real_part, imag_part = complex_times(
        real_part, imag_part, cos_table[None, :, None, None, :], -sin_table[None, :, None, None, :]
    )
    cos_table, sin_table = unit_circle(within[:, None] * within[None, :], positions)
    return complex_einsum("nj,rmbhj->rmbhn", cos_table, -sin_table, real_part, imag_part)


def inverse_rows(real_part, imag_part, frequencies, length):
    column_count, positions = (real_part.shape[1], real_part.shape[4])
    blocks, within, offsets = sequence_offsets(column_count, positions)
    cos_table, sin_table = unit_circle(within[:, None] * within[None, :], positions)
    real_part, imag_part = complex_einsum(
        "jn,rmbhn->rmbhj", cos_table, sin_table, real_part, imag_part
    )
    cos_table, sin_table = unit_circle(blocks[:, None] * within[None, :], column_count * positions)
    real_part, imag_part = complex_times(
        real_part, imag_part, cos_table[None, :, None, None, :], sin_table[None, :, None, None, :]
    )
    cos_table, sin_table = unit_circle(blocks[:, None] * blocks[None, :], column_count)
    real_part, imag_part = complex_einsum(
        "cm,rmbhj->rcbhj", cos_table, sin_table, real_part, imag_part
    )
    cos_table, sin_table = unit_circle(frequencies[:, None, None] * offsets[None], length)
    return complex_times(
        real_part, imag_part, cos_table[:, :, None, None, :], sin_table[:, :, None, None, :]
    )


def row_transform(operand, frequencies, sources, period):
    cos_table, sin_table = unit_circle(frequencies[:, None] * sources[None, :], period)
    imag_matrix = -sin_table
    flipped = unit_circle(period // 2 * sources[None, :], period)[0]
    imag_matrix = jnp.where(frequencies[:, None] == 0, flipped, imag_matrix)
    return (
        jnp.dot(cos_table, operand, precision=HIGHEST_PRECISION),
        jnp.dot(imag_matrix, operand, precision=HIGHEST_PRECISION),
    )


def row_inverse(real_part, imag_part, frequencies, rows_count, period, length):
    targets = jnp.arange(rows_count, dtype=jnp.int32)
    cos_table, sin_table = unit_circle(targets[:, None] * frequencies[None, :], period)
    real_matrix = cos_table / length
    imag_matrix = -sin_table / length
    flipped = unit_circle(period // 2 * targets[:, None], period)[0]
    head_row = frequencies[None, :] == 0
    real_matrix = jnp.where(head_row, 1.0, 2.0 * cos_table) / length
    imag_matrix = jnp.where(head_row, flipped, -2.0 * sin_table) / length
    return jnp.dot(real_matrix, real_part, precision=HIGHEST_PRECISION) + jnp.dot(
        imag_matrix, imag_part, precision=HIGHEST_PRECISION
    )


def unpack_head(real_part, imag_part, first_device):
    head_row = (jnp.arange(real_part.shape[0]) == 0)[:, None, None, None, None] & first_device
    extra_row = jnp.where(first_device, imag_part[:1], 0.0)
    cleared = jnp.where(head_row, 0.0, imag_part)
    return (
        jnp.concatenate([real_part, extra_row], axis=0),
        jnp.concatenate([cleared, jnp.zeros_like(extra_row)], axis=0),
    )


def pack_head(real_part, imag_part, first_device):
    head_imag = jnp.where(first_device, real_part[-1:], imag_part[:1])
    return (real_part[:-1], jnp.concatenate([head_imag, imag_part[1:-1]], axis=0))


def spectral_middle(signal, kernel, sequences, positions, share, column_index, send_out, send_back):
    rows_count = signal.shape[0]
    period = 2 * rows_count
    column_count = lax.axis_size("col")
    length = period * column_count * positions
    local_rows = rows_count // column_count
    frequencies = jnp.arange(rows_count, dtype=jnp.int32)
    signal_sources = jnp.arange(rows_count, dtype=jnp.int32)
    kernel_index = jnp.arange(period, dtype=jnp.int32)
    kernel_sources = kernel_index % 2 * rows_count + kernel_index // 2
    signal_real, signal_imag = row_transform(signal, frequencies, signal_sources, period)
    kernel_real, kernel_imag = row_transform(kernel, frequencies, kernel_sources, period)
    moved = send_out(
        signal_real[:, None], signal_imag[:, None], kernel_real[:, None], kernel_imag[:, None]
    )
    signal_shape = (local_rows, column_count, sequences, share, positions)
    kernel_shape = (local_rows, column_count, 1, share, positions)
    signal_real = moved[0].reshape(signal_shape)
    signal_imag = moved[1].reshape(signal_shape)
    kernel_real = moved[2].reshape(kernel_shape)
    kernel_imag = moved[3].reshape(kernel_shape)
    local_freq = column_index * local_rows + jnp.arange(local_rows, dtype=jnp.int32)
    first_device = column_index == 0
    signal_real, signal_imag = unpack_head(signal_real, signal_imag, first_device)
    kernel_real, kernel_imag = unpack_head(kernel_real, kernel_imag, first_device)
    local_freq = jnp.concatenate([local_freq, jnp.full((1,), rows_count, jnp.int32)])
    signal_real, signal_imag = forward_rows(signal_real, signal_imag, local_freq, length)
    kernel_real, kernel_imag = forward_rows(kernel_real, kernel_imag, local_freq, length)
    product_real, product_imag = complex_times(signal_real, signal_imag, kernel_real, kernel_imag)
    product_real, product_imag = inverse_rows(product_real, product_imag, local_freq, length)
    product_real, product_imag = pack_head(product_real, product_imag, first_device)
    returned = send_back(product_real, product_imag)
    columns = sequences * share * positions
    return row_inverse(
        returned[0].reshape(rows_count, columns),
        returned[1].reshape(rows_count, columns),
        frequencies,
        rows_count,
        period,
        length,
    )


def local(streams, filter_taps, short_taps, skip_gain, out_weight):
    sequences, positions, channels = (streams.shape[1], streams.shape[2], streams.shape[3])
    rows_count = lax.axis_size("row")
    share = channels // rows_count
    column_index = lax.axis_index("col")
    padded = with_halo(streams, ((("row", "col"), 2),), 1)
    smoothed = (
        short_taps[:, 0][:, None, None, :] * padded[:, :, :-2]
        + short_taps[:, 1][:, None, None, :] * padded[:, :, 1:-1]
        + short_taps[:, 2][:, None, None, :] * padded[:, :, 2:]
    )
    gated = smoothed[2] * smoothed[1]
    gated_lanes = jnp.transpose(gated, (0, 2, 1))[None]
    taps_lanes = jnp.transpose(filter_taps, (0, 2, 1))[:, None]
    by_channel, kernel_channel = (
        lax.all_to_all(gated_lanes, "row", split_axis=2, concat_axis=0, tiled=True),
        lax.all_to_all(taps_lanes, "row", split_axis=2, concat_axis=0, tiled=True),
    )
    signal = by_channel.reshape(rows_count, sequences * share * positions)
    kernel = kernel_channel.reshape(2 * rows_count, share * positions)

    def send_out(part_one, part_two, part_three, part_four):
        return (
            lax.all_to_all(part_one, "col", split_axis=0, concat_axis=1, tiled=True),
            lax.all_to_all(part_two, "col", split_axis=0, concat_axis=1, tiled=True),
            lax.all_to_all(part_three, "col", split_axis=0, concat_axis=1, tiled=True),
            lax.all_to_all(part_four, "col", split_axis=0, concat_axis=1, tiled=True),
        )

    def send_back(part_one, part_two):
        return (
            lax.all_to_all(part_one, "col", split_axis=1, concat_axis=0, tiled=True),
            lax.all_to_all(part_two, "col", split_axis=1, concat_axis=0, tiled=True),
        )

    spatial = spectral_middle(
        signal, kernel, sequences, positions, share, column_index, send_out, send_back
    )
    returned = lax.all_to_all(
        spatial.reshape(rows_count, sequences, share, positions),
        "row",
        split_axis=0,
        concat_axis=2,
        tiled=True,
    )
    convolved = jnp.transpose(returned[0], (0, 2, 1))
    mixed = ((convolved + skip_gain * gated) * smoothed[0]).astype(jnp.bfloat16)
    flattened = mixed.reshape(sequences * positions, channels)
    mean_square = jnp.mean(jnp.square(flattened.astype(jnp.float32)), axis=-1, keepdims=True)
    product = jnp.dot(flattened, out_weight, preferred_element_type=jnp.float32)
    scaled = (product * lax.rsqrt(mean_square + EPSILON)).astype(jnp.bfloat16)
    return scaled.reshape(sequences, positions, out_weight.shape[1])


def solution(mesh):
    in_specs = (P(None, None, ("row", "col"), None), P(None, ("row", "col"), None), P(), P(), P())
    out_specs = P(None, ("row", "col"), None)
    return jax.shard_map(local, mesh=mesh, in_specs=in_specs, out_specs=out_specs, check_vma=False)
```

profile of v0, /device:TPU:0, one launch (start us, length us, event | category | flops | bytes accessed | tf_op | source)
XLA Modules:
  0.0 156.4 jit_solution(409331134302281843)
XLA Ops:
  0.0 0.8 fusion.331
  1.1 1.3 collective-permute-start.1
  2.7 5.5 %collective-permute-start = (bf16[3,1,1,512]{2,3,1,0:T(8,128)(2,1)S(1)}, bf16[3,1,1,512]{2,3,1,0:T(8,128)(2,1)S(1)}, u32[]{:S(2)}, u32[]{:S(2)}) collective-permute-start(bf16[3,1,1,512]{2,3,1,0:T(8,128)(2,1)S(1)} %copy.51), channel_id=1, source_target_pairs={{0,1},{1,2},{2,3},{3,4},{4,5},{5,6},{6,7},{7,8},{8,9},{9,10},{10,1... | collective-permute-start | bytes 9224 | tf_op jit(solution)/shard_map/ppermute | solution.py:20
  8.3 0.9 fusion.332
  9.2 1.2 copy.52
  10.5 5.4 %collective-permute-done.1 = bf16[3,1,1,512]{2,3,1,0:T(8,128)(2,1)S(1)} collective-permute-done((bf16[3,1,1,512]{2,3,1,0:T(8,128)(2,1)S(1)}, bf16[3,1,1,512]{2,3,1,0:T(8,128)(2,1)S(1)}, u32[]{:S(2)}, u32[]{:S(2)}) %collective-permute-start.1) | collective-permute-done | bytes 3104 | tf_op jit(solution)/shard_map/ppermute | solution.py:22
  15.9 5.1 %collective-permute-done = bf16[3,1,1,512]{2,3,1,0:T(8,128)(2,1)S(1)} collective-permute-done((bf16[3,1,1,512]{2,3,1,0:T(8,128)(2,1)S(1)}, bf16[3,1,1,512]{2,3,1,0:T(8,128)(2,1)S(1)}, u32[]{:S(2)}, u32[]{:S(2)}) %collective-permute-start) | collective-permute-done | bytes 3104 | tf_op jit(solution)/shard_map/ppermute | solution.py:20
  21.1 1.1 multiply_add_fusion
  22.2 0.7 slice_multiply_fusion
  22.9 7.9 %all-to-all-start = ((f32[1,1,512,128]{3,1,0,2:T(1,128)}), f32[1,1,512,128]{3,1,0,2:T(1,128)S(1)}, u32[]{:S(2)}, u32[]{:S(2)}) async-start(f32[1,1,512,128]{3,1,0,2:T(1,128)} %bitcast.3), calls=%async_computation | async-start | bytes 524288 | tf_op jit(solution)/shard_map/all_to_all | solution.py:196
  30.8 1.0 copy.66
  32.0 8.5 %all-to-all-done = f32[1,1,512,128]{3,1,0,2:T(1,128)S(1)} async-done(((f32[1,1,512,128]{3,1,0,2:T(1,128)}), f32[1,1,512,128]{3,1,0,2:T(1,128)S(1)}, u32[]{:S(2)}, u32[]{:S(2)}) %all-to-all-start) | async-done | bytes 262176 | tf_op jit(solution)/shard_map/all_to_all | solution.py:196
  40.5 0.5 broadcast.948
  41.0 1.2 reduce.3
  42.7 1.0 copy.59
  43.7 3.4 %all-to-all-start.2 = ((f32[8,1,8192]{2,1,0:T(1,128)}), f32[8,1,8192]{2,1,0:T(1,128)S(1)}, u32[]{:S(2)}, u32[]{:S(2)}) async-start(f32[8,1,8192]{2,1,0:T(1,128)} %copy.59), calls=%async_computation.2 | async-start | bytes 524288 | tf_op jit(solution)/shard_map/all_to_all | solution.py:205
  47.6 1.0 copy.57
  48.6 3.9 %all-to-all-done.2 = f32[8,1,8192]{2,1,0:T(1,128)S(1)} async-done(((f32[8,1,8192]{2,1,0:T(1,128)}), f32[8,1,8192]{2,1,0:T(1,128)S(1)}, u32[]{:S(2)}, u32[]{:S(2)}) %all-to-all-start.2) | async-done | bytes 262176 | tf_op jit(solution)/shard_map/all_to_all | solution.py:205
  52.5 3.4 %all-to-all-start.1 = ((f32[8,1,8192]{2,1,0:T(1,128)}), f32[8,1,8192]{2,1,0:T(1,128)S(1)}, u32[]{:S(2)}, u32[]{:S(2)}) async-start(f32[8,1,8192]{2,1,0:T(1,128)} %copy.57), calls=%async_computation.1 | async-start | bytes 524288 | tf_op jit(solution)/shard_map/all_to_all | solution.py:204
  56.0 5.2 %all-to-all-done.1 = f32[8,1,8192]{2,1,0:T(1,128)S(1)} async-done(((f32[8,1,8192]{2,1,0:T(1,128)}), f32[8,1,8192]{2,1,0:T(1,128)S(1)}, u32[]{:S(2)}, u32[]{:S(2)}) %all-to-all-start.1) | async-done | bytes 262176 | tf_op jit(solution)/shard_map/all_to_all | solution.py:204
  61.2 3.5 %all-to-all-start.3 = ((f32[2,1,512,128]{3,0,1,2:T(2,128)}), f32[2,1,512,128]{3,0,1,2:T(2,128)S(1)}, u32[]{:S(2)}, u32[]{:S(2)}) async-start(f32[2,1,512,128]{3,0,1,2:T(2,128)} %bitcast.34), calls=%async_computation.3 | async-start | bytes 1048576 | tf_op jit(solution)/shard_map/all_to_all | solution.py:197
  64.9 15.1 %all-to-all-done.3 = f32[2,1,512,128]{3,0,1,2:T(2,128)S(1)} async-done(((f32[2,1,512,128]{3,0,1,2:T(2,128)}), f32[2,1,512,128]{3,0,1,2:T(2,128)S(1)}, u32[]{:S(2)}, u32[]{:S(2)}) %all-to-all-start.3) | async-done | bytes 524320 | tf_op jit(solution)/shard_map/all_to_all | solution.py:197
  80.0 0.7 convolution_bitcast_fusion
  80.7 1.0 copy.71
  81.7 3.4 %all-to-all-start.5 = ((f32[8,1,8192]{2,1,0:T(1,128)}), f32[8,1,8192]{2,1,0:T(1,128)S(1)}, u32[]{:S(2)}, u32[]{:S(2)}) async-start(f32[8,1,8192]{2,1,0:T(1,128)} %copy.71), calls=%async_computation.5 | async-start | bytes 524288 | tf_op jit(solution)/shard_map/all_to_all | solution.py:207
  85.3 0.7 convolution_bitcast_fusion.1
  85.9 1.0 copy.69
  86.9 3.5 %all-to-all-done.5 = f32[8,1,8192]{2,1,0:T(1,128)S(1)} async-done(((f32[8,1,8192]{2,1,0:T(1,128)}), f32[8,1,8192]{2,1,0:T(1,128)S(1)}, u32[]{:S(2)}, u32[]{:S(2)}) %all-to-all-start.5) | async-done | bytes 262176 | tf_op jit(solution)/shard_map/all_to_all | solution.py:207
  90.4 3.6 %all-to-all-start.4 = ((f32[8,1,8192]{2,1,0:T(1,128)}), f32[8,1,8192]{2,1,0:T(1,128)S(1)}, u32[]{:S(2)}, u32[]{:S(2)}) async-start(f32[8,1,8192]{2,1,0:T(1,128)} %copy.69), calls=%async_computation.4 | async-start | bytes 524288 | tf_op jit(solution)/shard_map/all_to_all | solution.py:206
  94.2 5.0 %all-to-all-done.4 = f32[8,1,8192]{2,1,0:T(1,128)S(1)} async-done(((f32[8,1,8192]{2,1,0:T(1,128)}), f32[8,1,8192]{2,1,0:T(1,128)S(1)}, u32[]{:S(2)}, u32[]{:S(2)}) %all-to-all-start.4) | async-done | bytes 262176 | tf_op jit(solution)/shard_map/all_to_all | solution.py:206
  100.0 0.9 fusion.48
  100.9 0.9 fusion.52
  101.8 0.9 fusion.54
  102.7 0.9 fusion.58
  103.6 0.9 fusion.4
  104.5 0.9 fusion.5
  105.5 0.9 fusion.6
  106.4 1.3 add_bitcast_fusion
  107.6 0.7 fusion.21
  108.4 0.7 fusion.25
  109.1 0.7 convolution_add_fusion.3
  109.8 0.7 convolution_subtract_fusion.2
  110.5 0.9 fusion.27
  111.5 0.7 fusion.31
  112.2 0.7 convolution_subtract_fusion.4
  112.9 0.8 multiply_subtract_fusion.2
  113.7 0.7 fusion.71
  114.4 0.7 fusion.69
  115.1 0.7 convolution_subtract_fusion.1
  115.8 0.8 multiply_subtract_fusion.1
  116.6 1.0 fusion.37
  117.7 1.0 fusion.33
  118.7 1.0 fusion.3
  119.8 1.2 multiply_add_fusion.1
  121.0 0.7 copy.86
  121.7 3.4 %all-to-all-start.6 = ((f32[2,4,1,64,128]{4,3,0,2,1:T(8,128)}), f32[2,4,1,64,128]{4,3,0,2,1:T(8,128)S(1)}, u32[]{:S(2)}, u32[]{:S(2)}) async-start(f32[2,4,1,64,128]{4,3,0,2,1:T(8,128)} %copy.86), calls=%async_computation.6 | async-start | bytes 524288 | tf_op jit(solution)/shard_map/all_to_all | solution.py:212
  125.2 0.7 copy.87
  125.9 4.5 %all-to-all-done.6 = f32[2,4,1,64,128]{4,3,0,2,1:T(8,128)S(1)} async-done(((f32[2,4,1,64,128]{4,3,0,2,1:T(8,128)}), f32[2,4,1,64,128]{4,3,0,2,1:T(8,128)S(1)}, u32[]{:S(2)}, u32[]{:S(2)}) %all-to-all-start.6) | async-done | bytes 262176 | tf_op jit(solution)/shard_map/all_to_all | solution.py:212
  130.4 3.4 %all-to-all-start.7 = ((f32[2,4,1,64,128]{4,3,0,2,1:T(8,128)}), f32[2,4,1,64,128]{4,3,0,2,1:T(8,128)S(1)}, u32[]{:S(2)}, u32[]{:S(2)}) async-start(f32[2,4,1,64,128]{4,3,0,2,1:T(8,128)} %copy.87), calls=%async_computation.7 | async-start | bytes 524288 | tf_op jit(solution)/shard_map/all_to_all | solution.py:213
  133.8 0.5 fusion.41
  134.3 4.8 %all-to-all-done.7 = f32[2,4,1,64,128]{4,3,0,2,1:T(8,128)S(1)} async-done(((f32[2,4,1,64,128]{4,3,0,2,1:T(8,128)}), f32[2,4,1,64,128]{4,3,0,2,1:T(8,128)S(1)}, u32[]{:S(2)}, u32[]{:S(2)}) %all-to-all-start.7) | async-done | bytes 262176 | tf_op jit(solution)/shard_map/all_to_all | solution.py:213
  139.2 0.5 fusion.8
  139.7 12.5 %all_to_all.123 = f32[8,1,64,128]{3,2,1,0:T(8,128)S(1)} all-to-all(f32[8,1,64,128]{3,2,1,0:T(8,128)S(1)} %copy.88), channel_id=1, replica_groups=mesh['row'=8,'col'=4] {'row'}, dimensions={0} | all-to-all | bytes 524288 | tf_op jit(solution)/shard_map/all_to_all | solution.py:219
  152.4 3.9 %fusion.1 = bf16[1,128,4096]{2,1,0:T(8,128)(2,1)} fusion(bf16[128,512]{0,1:T(8,128)(2,1)S(1)} %get-tuple-element.6, bf16[512,4096]{1,0:T(8,128)(2,1)} %param.9, f32[128]{0:T(128)S(1)} %add_rsqrt_fusion), kind=kOutput, calls=%fused_computation.7 | convolution fusion | flops 537919488 | bytes 5374464 | tf_op jit(solution)/shard_map/dot_general | solution.py:230
  (42 shorter events, 3.6 us)
Async XLA Ops:
  0.0 30.8 %copy-start = (f32[2,128,512]{2,1,0:T(8,128)S(1)}, f32[2,128,512]{2,1,0:T(8,128)}, u32[]{:S(2)}) copy-start(f32[2,128,512]{2,1,0:T(8,128)} %param.6) | copy-start | bytes 1572868
  1.1 14.8 %collective-permute-start.1 = (bf16[3,1,1,512]{2,3,1,0:T(8,128)(2,1)S(1)}, bf16[3,1,1,512]{2,3,1,0:T(8,128)(2,1)S(1)}, u32[]{:S(2)}, u32[]{:S(2)}) collective-permute-start(bf16[3,1,1,512]{2,3,1,0:T(8,128)(2,1)S(1)} %copy.54), channel_id=1, source_target_pairs={{1,0},{2,1},{3,2},{4,3},{5,4},{6,5},{7,6},{8,7},{9,8},{10,9},{11,1... | collective-permute-start | bytes 9224 | tf_op jit(solution)/shard_map/ppermute | solution.py:22
  2.7 18.4 %collective-permute-start = (bf16[3,1,1,512]{2,3,1,0:T(8,128)(2,1)S(1)}, bf16[3,1,1,512]{2,3,1,0:T(8,128)(2,1)S(1)}, u32[]{:S(2)}, u32[]{:S(2)}) collective-permute-start(bf16[3,1,1,512]{2,3,1,0:T(8,128)(2,1)S(1)} %copy.51), channel_id=1, source_target_pairs={{0,1},{1,2},{2,3},{3,4},{4,5},{5,6},{6,7},{7,8},{8,9},{9,10},{10,1... | collective-permute-start | bytes 9224 | tf_op jit(solution)/shard_map/ppermute | solution.py:20
  22.9 17.6 %all-to-all-start = ((f32[1,1,512,128]{3,1,0,2:T(1,128)}), f32[1,1,512,128]{3,1,0,2:T(1,128)S(1)}, u32[]{:S(2)}, u32[]{:S(2)}) async-start(f32[1,1,512,128]{3,1,0,2:T(1,128)} %bitcast.3), calls=%async_computation | async-start | bytes 524288 | tf_op jit(solution)/shard_map/all_to_all | solution.py:196
  43.7 8.8 %all-to-all-start.2 = ((f32[8,1,8192]{2,1,0:T(1,128)}), f32[8,1,8192]{2,1,0:T(1,128)S(1)}, u32[]{:S(2)}, u32[]{:S(2)}) async-start(f32[8,1,8192]{2,1,0:T(1,128)} %copy.59), calls=%async_computation.2 | async-start | bytes 524288 | tf_op jit(solution)/shard_map/all_to_all | solution.py:205
  52.5 8.8 %all-to-all-start.1 = ((f32[8,1,8192]{2,1,0:T(1,128)}), f32[8,1,8192]{2,1,0:T(1,128)S(1)}, u32[]{:S(2)}, u32[]{:S(2)}) async-start(f32[8,1,8192]{2,1,0:T(1,128)} %copy.57), calls=%async_computation.1 | async-start | bytes 524288 | tf_op jit(solution)/shard_map/all_to_all | solution.py:204
  61.2 18.8 %all-to-all-start.3 = ((f32[2,1,512,128]{3,0,1,2:T(2,128)}), f32[2,1,512,128]{3,0,1,2:T(2,128)S(1)}, u32[]{:S(2)}, u32[]{:S(2)}) async-start(f32[2,1,512,128]{3,0,1,2:T(2,128)} %bitcast.34), calls=%async_computation.3 | async-start | bytes 1048576 | tf_op jit(solution)/shard_map/all_to_all | solution.py:197
  81.7 8.8 %all-to-all-start.5 = ((f32[8,1,8192]{2,1,0:T(1,128)}), f32[8,1,8192]{2,1,0:T(1,128)S(1)}, u32[]{:S(2)}, u32[]{:S(2)}) async-start(f32[8,1,8192]{2,1,0:T(1,128)} %copy.71), calls=%async_computation.5 | async-start | bytes 524288 | tf_op jit(solution)/shard_map/all_to_all | solution.py:207
  90.4 8.8 %all-to-all-start.4 = ((f32[8,1,8192]{2,1,0:T(1,128)}), f32[8,1,8192]{2,1,0:T(1,128)S(1)}, u32[]{:S(2)}, u32[]{:S(2)}) async-start(f32[8,1,8192]{2,1,0:T(1,128)} %copy.69), calls=%async_computation.4 | async-start | bytes 524288 | tf_op jit(solution)/shard_map/all_to_all | solution.py:206
  119.7 32.5 %copy-start.1 = (f32[512]{0:T(512)S(1)}, f32[512]{0:T(512)}, u32[]{:S(2)}) copy-start(f32[512]{0:T(512)} %param.8) | copy-start | bytes 6148
  121.7 8.8 %all-to-all-start.6 = ((f32[2,4,1,64,128]{4,3,0,2,1:T(8,128)}), f32[2,4,1,64,128]{4,3,0,2,1:T(8,128)S(1)}, u32[]{:S(2)}, u32[]{:S(2)}) async-start(f32[2,4,1,64,128]{4,3,0,2,1:T(8,128)} %copy.86), calls=%async_computation.6 | async-start | bytes 524288 | tf_op jit(solution)/shard_map/all_to_all | solution.py:212
  130.4 8.8 %all-to-all-start.7 = ((f32[2,4,1,64,128]{4,3,0,2,1:T(8,128)}), f32[2,4,1,64,128]{4,3,0,2,1:T(8,128)S(1)}, u32[]{:S(2)}, u32[]{:S(2)}) async-start(f32[2,4,1,64,128]{4,3,0,2,1:T(8,128)} %copy.87), calls=%async_computation.7 | async-start | bytes 524288 | tf_op jit(solution)/shard_map/all_to_all | solution.py:213
where the time goes:
time: 157 us; the launch traced here: 156 us
  waiting for transfers between devices  61.1 us (39%)
  starting transfers between devices  38.9 us (25%)
  matrix products  27.7 us (18%)
  blocking collectives  12.5 us (8%)
  local copies, waits for them, and re-layouts  11.1 us (7%)
  other arithmetic  4.41 us (3%)
    dot_general x24, matrix products, single(): return jnp.einsum(formula, matrix, operand, precision=HIGHEST_PRECISION)  20.7 us
    all_to_all x1, waiting for transfers between devices, local(): lax.all_to_all(taps_lanes, 'row', split_axis=2, concat_axis=0, tiled=True)  15.1 us
    all_to_all x1, blocking collectives, local(): lax.all_to_all(spatial.reshape(rows_count, sequences, share, positions),...  12.5 us
    all_to_all x1, waiting for transfers between devices, local(): lax.all_to_all(gated_lanes, 'row', split_axis=2, concat_axis=0, tiled=True)  8.52 us
    all_to_all x1, starting transfers between devices, local(): lax.all_to_all(gated_lanes, 'row', split_axis=2, concat_axis=0, tiled=True)  7.94 us
    ppermute x1, starting transfers between devices, with_halo(): lax.ppermute(tail, axis, [(i, (i + 1) % count) for i in range(ends)])  5.52 us
    ppermute x1, waiting for transfers between devices, with_halo(): lax.ppermute(head, axis, [((i + 1) % count, i) for i in range(ends)])  5.44 us
    all_to_all x1, waiting for transfers between devices, send_out(): lax.all_to_all(part_one, 'col', split_axis=0, concat_axis=1, tiled=True)  5.17 us
  transfers between devices with their start and end apart: 10, of which 10 were waited for; matrix products, arithmetic and copies ran while one was open for 6% of the time, Pallas kernels for 0%

commit v1 on v0

--- a/solution.py
+++ b/solution.py
@@ -1,8 +1,12 @@
+import functools
 import math
 
 import jax
 import jax.numpy as jnp
+import numpy as np
 from jax import lax
+from jax.experimental import pallas as pl
+from jax.experimental.pallas import tpu as pltpu
 from jax.sharding import PartitionSpec as P
 
 HIGHEST_PRECISION = lax.Precision.HIGHEST
@@ -232,7 +236,270 @@
     return scaled.reshape(sequences, positions, out_weight.shape[1])
 
 
+def split_pair(value):
+    high = value.astype(jnp.bfloat16)
+    return high, (value - high.astype(jnp.float32)).astype(jnp.bfloat16)
+
+
+def split_pair_host(table):
+    table = np.asarray(table, np.float32)
+    high = table.astype(jnp.bfloat16)
+    return high, (table - high.astype(np.float32)).astype(jnp.bfloat16)
+
+
+def host_tables(devices, share, positions):
+    blocks = 2 * devices
+    length = blocks * positions
+    first = np.arange(devices + 1)
+    source = np.arange(devices)
+    angle = 2.0 * np.pi / blocks * (first[:, None] * source[None, :] % blocks)
+    rows = np.concatenate([np.cos(angle), -np.sin(angle[1:devices])])
+    outer = np.kron(rows, np.eye(share))
+    within = np.arange(positions)
+    angle = 2.0 * np.pi / length * (first[:, None] * within[None, :] % length)
+    twiddle = np.stack([np.cos(angle), np.sin(angle)])[:, :, None, :].astype(np.float32)
+    angle = 2.0 * np.pi / positions * (within[:, None] * within[None, :] % positions)
+    cos_table, sin_table = np.cos(angle), np.sin(angle)
+    inner = np.block([[cos_table, -sin_table], [sin_table, cos_table]])
+    return (*split_pair_host(outer), *split_pair_host(inner), twiddle)
+
+
+def dot32(left, right, dims=((1,), (0,))):
+    return lax.dot_general(left, right, (dims, ((), ())), preferred_element_type=jnp.float32)
+
+
+def whole_kernel(
+    axes, sizes, streams_hbm, taps_hbm, short_ref, gain_ref, weight_hbm, outer_high_hbm, outer_low_hbm,
+    inner_high_ref, inner_low_ref, twiddle_ref, out_ref,
+    streams, taps, weight, outer_high, outer_low, halo_before, halo_after,
+    taps_send, taps_recv, gated_send, gated_recv, back_send, back_recv,
+    local_sems, halo_sems, send_sems, recv_sems,
+):
+    devices, share, positions, channels = sizes
+    columns = lax.axis_size(axes[1])
+    me = lax.axis_index(axes[0]) * columns + lax.axis_index(axes[1])
+    mesh_id = pl.DeviceIdType.MESH
+
+    def place(device):
+        return (lax.div(device, columns), lax.rem(device, columns))
+
+    def partner(step):
+        return lax.rem(me + step, devices)
+
+    loads = [
+        pltpu.make_async_copy(source, target, local_sems.at[i])
+        for i, (source, target) in enumerate(
+            [
+                (taps_hbm, taps),
+                (streams_hbm, streams),
+                (outer_high_hbm, outer_high),
+                (outer_low_hbm, outer_low),
+                (weight_hbm, weight),
+            ]
+        )
+    ]
+    for load in loads:
+        load.start()
+    barrier = pltpu.get_barrier_semaphore()
+    for step in range(1, devices):
+        pl.semaphore_signal(barrier, inc=1, device_id=place(partner(step)), device_id_type=mesh_id)
+
+    loads[0].wait()
+    for half in range(2):
+        turned = jnp.transpose(taps[half]).astype(jnp.bfloat16)
+        taps_send[half] = turned.reshape(devices, share, positions)
+    taps_recv[:, me] = taps_send[:, me]
+    pl.semaphore_wait(barrier, devices - 1)
+
+    edge = halo_before.shape[1]
+    halo_copies = [
+        pltpu.make_async_remote_copy(
+            src_ref=streams_hbm.at[:, pl.ds(positions - edge, edge)],
+            dst_ref=halo_before,
+            send_sem=halo_sems.at[0],
+            recv_sem=halo_sems.at[1],
+            device_id=place(partner(1)),
+            device_id_type=mesh_id,
+        ),
+        pltpu.make_async_remote_copy(
+            src_ref=streams_hbm.at[:, pl.ds(0, edge)],
+            dst_ref=halo_after,
+            send_sem=halo_sems.at[2],
+            recv_sem=halo_sems.at[3],
+            device_id=place(partner(devices - 1)),
+            device_id_type=mesh_id,
+        ),
+    ]
+    for copy in halo_copies:
+        copy.start()
+
+    def exchange(kind, source, target):
+        copies = []
+        for step in range(1, devices):
+            device = partner(step)
+            copies.append(
+                pltpu.make_async_remote_copy(
+                    src_ref=source(device),
+                    dst_ref=target,
+                    send_sem=send_sems.at[kind, step],
+                    recv_sem=recv_sems.at[kind, step],
+                    device_id=place(device),
+                    device_id_type=mesh_id,
+                )
+            )
+        for copy in copies:
+            copy.start()
+        return copies
+
+    taps_copies = exchange(0, lambda device: taps_send.at[:, device], taps_recv.at[:, me])
+
+    loads[1].wait()
+    for copy in halo_copies:
+        copy.wait()
+    row = lax.broadcasted_iota(jnp.int32, (positions, channels), 0)
+    smoothed = []
+    for s in range(3):
+        middle = streams[s].astype(jnp.float32)
+        before = jnp.where(me > 0, halo_before[s].astype(jnp.float32)[edge - 1 : edge], 0.0)
+        after = jnp.where(me < devices - 1, halo_after[s].astype(jnp.float32)[:1], 0.0)
+        previous = jnp.where(row == 0, before, pltpu.roll(middle, 1, 0))
+        following = jnp.where(row == positions - 1, after, pltpu.roll(middle, positions - 1, 0))
+        smoothed.append(
+            short_ref[s, 0:1] * previous + short_ref[s, 1:2] * middle + short_ref[s, 2:3] * following
+        )
+    gated = smoothed[2] * smoothed[1]
+    gated_send[...] = jnp.transpose(gated).astype(jnp.bfloat16).reshape(devices, share, positions)
+    gated_recv[me] = gated_send[me]
+    gated_copies = exchange(1, lambda device: gated_send.at[device], gated_recv.at[me])
+
+    groups = devices + 1
+    rows = groups * share
+    shape = (groups, share, positions)
+    cos_table = jnp.broadcast_to(twiddle_ref[0], shape).reshape(rows, positions)
+    sin_table = jnp.broadcast_to(twiddle_ref[1], shape).reshape(rows, positions)
+    inner_high, inner_low = inner_high_ref[...], inner_low_ref[...]
+
+    def inner_product(operand, dims):
+        high, low = split_pair(operand)
+        return dot32(high, inner_high, dims) + (dot32(low, inner_high, dims) + dot32(high, inner_low, dims))
+
+    def outer_product(operand):
+        return dot32(outer_high[...], operand) + dot32(outer_low[...], operand)
+
+    def spectrum(parts):
+        blank = jnp.zeros((share, positions), jnp.float32)
+        real_part = parts[:rows]
+        imag_part = jnp.concatenate([blank, parts[rows:], blank], axis=0)
+        turned_real = real_part * cos_table + imag_part * sin_table
+        turned_imag = imag_part * cos_table - real_part * sin_table
+        both = inner_product(jnp.concatenate([turned_real, turned_imag], axis=1), ((1,), (0,)))
+        return both[:, :positions], both[:, positions:]
+
+    loads[2].wait()
+    loads[3].wait()
+    for copy in taps_copies:
+        copy.wait_recv()
+    halves = jnp.concatenate(
+        [taps_recv[half].reshape(devices * share, positions) for half in range(2)], axis=1
+    )
+    halves = outer_product(halves)
+    part_row = lax.broadcasted_iota(jnp.int32, (2 * devices * share, positions), 0) // share
+    frequency = jnp.where(part_row > devices, part_row - devices, part_row)
+    second = halves[:, positions:]
+    kernel_parts = halves[:, :positions] + jnp.where(frequency % 2 == 1, -second, second)
+    kernel_real, kernel_imag = spectrum(kernel_parts)
+
+    for copy in gated_copies:
+        copy.wait_recv()
+    signal_real, signal_imag = spectrum(outer_product(gated_recv[...].reshape(devices * share, positions)))
+    product_real, product_imag = complex_times(signal_real, signal_imag, kernel_real, kernel_imag)
+    both = inner_product(jnp.concatenate([product_real, product_imag], axis=1), ((1,), (1,)))
+    real_part, imag_part = both[:, :positions], both[:, positions:]
+    back_real = real_part * cos_table - imag_part * sin_table
+    back_imag = real_part * sin_table + imag_part * cos_table
+    scale = 1.0 / (2 * devices * positions)
+    ends = lax.broadcasted_iota(jnp.int32, (rows, positions), 0) // share % devices == 0
+    back_real = back_real * jnp.where(ends, scale, 2.0 * scale)
+    back_imag = back_imag * (2.0 * scale)
+    back = jnp.concatenate([back_real, back_imag[share : rows - share]], axis=0)
+    high, low = split_pair(back)
+    dims = ((0,), (0,))
+    spatial = dot32(outer_high[...], high, dims) + (
+        dot32(outer_high[...], low, dims) + dot32(outer_low[...], high, dims)
+    )
+    back_send[...] = spatial.astype(jnp.bfloat16).reshape(devices, share, positions)
+    back_recv[me] = back_send[me]
+    back_copies = exchange(2, lambda device: back_send.at[device], back_recv.at[me])
+    for copy in back_copies:
+        copy.wait_recv()
+    convolved = jnp.transpose(back_recv[...].reshape(channels, positions).astype(jnp.float32))
+    mixed = ((convolved + gain_ref[...] * gated) * smoothed[0]).astype(jnp.bfloat16)
+    mean_square = jnp.mean(jnp.square(mixed.astype(jnp.float32)), axis=-1, keepdims=True)
+    row_scale = lax.rsqrt(mean_square + EPSILON)
+    loads[4].wait()
+    out_ref[...] = (dot32(mixed, weight[...]) * row_scale).astype(jnp.bfloat16)
+    for copy in taps_copies + gated_copies + back_copies:
+        copy.wait_send()
+
+
+def exchanged_once(axes, streams, filter_taps, short_taps, skip_gain, out_weight):
+    positions, channels = streams.shape[2:]
+    width = out_weight.shape[1]
+    devices = lax.axis_size(axes[0]) * lax.axis_size(axes[1])
+    share = channels // devices
+    tables = host_tables(devices, share, positions)
+    half = (devices, share, positions)
+    edge = 16
+    anywhere = pl.BlockSpec(memory_space=pl.ANY)
+    vector = pl.BlockSpec(memory_space=pltpu.VMEM)
+    outer_shape = tables[0].shape
+    projected = pl.pallas_call(
+        functools.partial(whole_kernel, axes, (devices, share, positions, channels)),
+        out_shape=jax.ShapeDtypeStruct((positions, width), jnp.bfloat16),
+        in_specs=[anywhere, anywhere, vector, vector, anywhere, anywhere, anywhere, vector, vector, vector],
+        out_specs=vector,
+        scratch_shapes=[
+            pltpu.VMEM((3, positions, channels), jnp.bfloat16),
+            pltpu.VMEM((2, positions, channels), jnp.float32),
+            pltpu.VMEM((channels, width), jnp.bfloat16),
+            pltpu.VMEM(outer_shape, jnp.bfloat16),
+            pltpu.VMEM(outer_shape, jnp.bfloat16),
+            pltpu.VMEM((3, edge, channels), jnp.bfloat16),
+            pltpu.VMEM((3, edge, channels), jnp.bfloat16),
+            pltpu.VMEM((2, *half), jnp.bfloat16),
+            pltpu.VMEM((2, *half), jnp.bfloat16),
+            pltpu.VMEM(half, jnp.bfloat16),
+            pltpu.VMEM(half, jnp.bfloat16),
+            pltpu.VMEM(half, jnp.bfloat16),
+            pltpu.VMEM(half, jnp.bfloat16),
+            pltpu.SemaphoreType.DMA((5,)),
+            pltpu.SemaphoreType.DMA((4,)),
+            pltpu.SemaphoreType.DMA((3, devices)),
+            pltpu.SemaphoreType.DMA((3, devices)),
+        ],
+        compiler_params=pltpu.CompilerParams(collective_id=0, has_side_effects=True),
+    )(
+        streams.reshape(3, positions, channels),
+        filter_taps,
+        short_taps,
+        skip_gain.reshape(1, channels),
+        out_weight,
+        *(jnp.asarray(table) for table in tables),
+    )
+    return projected.reshape(1, positions, width)
+
+
+def local_any(axes, streams, *others):
+    sequences, positions, channels = streams.shape[1:]
+    devices = lax.axis_size(axes[0]) * lax.axis_size(axes[1])
+    tiled = channels % (16 * devices) == 0 and positions == 128 and devices * channels <= 2**15
+    if sequences == 1 and tiled and devices > 1:
+        return exchanged_once(axes, streams, *others)
+    return local(streams, *others)
+
+
 def solution(mesh):
     in_specs = (P(None, None, ("row", "col"), None), P(None, ("row", "col"), None), P(), P(), P())
     out_specs = P(None, ("row", "col"), None)
-    return jax.shard_map(local, mesh=mesh, in_specs=in_specs, out_specs=out_specs, check_vma=False)
+    body = functools.partial(local_any, ("row", "col"))
+    return jax.shard_map(body, mesh=mesh, in_specs=in_specs, out_specs=out_specs, check_vma=False)

time: 157 us -> 35.4 us (0.23)
  waiting for transfers between devices: 61.1 us -> 0 us
  starting transfers between devices: 38.9 us -> 0 us
  Pallas kernels: 0 us -> 32.9 us
  matrix products: 27.7 us -> 0 us
  blocking collectives: 12.5 us -> 0 us
  local copies, waits for them, and re-layouts: 11.1 us -> 2.29 us
  other arithmetic: 4.41 us -> 0 us
    all_to_all x8 -> x0, waiting for transfers between devices: 50.5 us -> none  [the longest x1 15.1 us: local(): lax.all_to_all(taps_lanes, 'row', split_axis=2, concat_axis=0, tiled=True)]
    pallas_call x0 -> x1, Pallas kernels: none -> 32.9 us  [exchanged_once(): pl.pallas_call(functools.partial(whole_kernel, axes, (devices, share, pos...]
    all_to_all x8 -> x0, starting transfers between devices: 32 us -> none  [the longest x1 7.94 us: local(): lax.all_to_all(gated_lanes, 'row', split_axis=2, concat_axis=0, tiled=True)]
    dot_general x31 -> x0, matrix products: 27.7 us -> none  [the longest x24 20.7 us: single(): return jnp.einsum(formula, matrix, operand, precision=HIGHEST_PRECISION)]
    all_to_all x1 -> x0, blocking collectives: 12.5 us -> none  [local(): lax.all_to_all(spatial.reshape(rows_count, sequences, share, positions),...]
    ppermute x2 -> x0, waiting for transfers between devices: 10.6 us -> none  [the longest x1 5.44 us: with_halo(): lax.ppermute(head, axis, [((i + 1) % count, i) for i in range(ends)])]
    ppermute x2 -> x0, starting transfers between devices: 6.82 us -> none  [the longest x1 5.52 us: with_halo(): lax.ppermute(tail, axis, [(i, (i + 1) % count) for i in range(ends)])]
    broadcast_in_dim x4 -> x0, local copies, waits for them, and re-layouts: 3.88 us -> none  [the longest x1 0.97 us: spectral_middle(): kernel_real[:, None]]
  transfers between devices with their start and end apart: 10 -> 0, of which waited for: 10 -> 0; matrix products, arithmetic and copies ran while one was open for 6% -> 0% of each run, Pallas kernels for 0% -> 0%
where the time goes in v1:
time: 35.4 us; the launch traced here: 35.2 us
  Pallas kernels  32.9 us (93%)
  local copies, waits for them, and re-layouts  2.29 us (6%)
    pallas_call x1, Pallas kernels, exchanged_once(): pl.pallas_call(functools.partial(whole_kernel, axes, (devices, share, pos...  32.9 us
    unnamed x1, local copies, waits for them, and re-layouts  2.29 us

profile of v1, /device:TPU:0, one launch (start us, length us, event | category | flops | bytes accessed | tf_op | source)
XLA Modules:
  0.0 35.2 jit_solution(16993346772790526183)
XLA Ops:
  0.0 32.9 %shard_map.100 = bf16[128,4096]{1,0:T(8,128)(2,1)} custom-call(bf16[3,128,512]{2,1,0:T(8,128)(2,1)} %bitcast.4, f32[2,128,512]{2,1,0:T(8,128)} %taps_hbm.1, f32[3,3,512]{2,1,0:T(4,128)} %short_ref.1, f32[1,512]{1,0:T(1,128)} %bitcast.5, bf16[512,4096]{1,0:T(8,128)(2,1)} %weight_hbm.1, bf16[1024,512]{1,0:T(8,128)(2,1)} %constant.10.clone.outer_high_hbm, ...), custom_call_target="tpu_custom_call" | custom-call | tf_op jit(solution)/shard_map/pallas_call | solution.py:456
  32.9 2.3 %copy.12 = bf16[1,128,4096]{2,1,0:T(8,128)(2,1)} copy(bf16[1,128,4096]{2,1,0:T(8,128)(2,1)} %bitcast.3) | data formatting | bytes 2097152

commit v2 on v1

--- a/solution.py
+++ b/solution.py
@@ -269,9 +269,10 @@
 
 
 def whole_kernel(
-    axes, sizes, streams_hbm, taps_hbm, short_ref, gain_ref, weight_hbm, outer_high_hbm, outer_low_hbm,
-    inner_high_ref, inner_low_ref, twiddle_ref, out_ref,
-    streams, taps, weight, outer_high, outer_low, halo_before, halo_after,
+    axes, sizes, streams_hbm, taps_hbm, short_hbm, gain_hbm, outer_high_hbm, outer_low_hbm,
+    inner_high_hbm, inner_low_hbm, twiddle_hbm, weight_hbm, mixed_ref, scale_ref, weight_ref,
+    streams, taps, short_ref, gain_ref, outer_high, outer_low, inner_high_ref, inner_low_ref, twiddle_ref,
+    edges, halo_before, halo_after,
     taps_send, taps_recv, gated_send, gated_recv, back_send, back_recv,
     local_sems, halo_sems, send_sems, recv_sems,
 ):
@@ -292,43 +293,47 @@
             [
                 (taps_hbm, taps),
                 (streams_hbm, streams),
+                (short_hbm, short_ref),
                 (outer_high_hbm, outer_high),
                 (outer_low_hbm, outer_low),
-                (weight_hbm, weight),
+                (inner_high_hbm, inner_high_ref),
+                (inner_low_hbm, inner_low_ref),
+                (twiddle_hbm, twiddle_ref),
+                (gain_hbm, gain_ref),
+                (weight_hbm, weight_ref),
             ]
         )
     ]
-    for load in loads:
+    barrier = pltpu.get_barrier_semaphore()
+    for load in loads[:3]:
         load.start()
-    barrier = pltpu.get_barrier_semaphore()
     for step in range(1, devices):
         pl.semaphore_signal(barrier, inc=1, device_id=place(partner(step)), device_id_type=mesh_id)
+    for load in loads[3:]:
+        load.start()
 
     loads[0].wait()
     for half in range(2):
         turned = jnp.transpose(taps[half]).astype(jnp.bfloat16)
         taps_send[half] = turned.reshape(devices, share, positions)
     taps_recv[:, me] = taps_send[:, me]
+    loads[1].wait()
+    for s in range(3):
+        middle = streams[s].astype(jnp.float32)
+        edges[0, s : s + 1] = middle[positions - 1 :]
+        edges[1, s : s + 1] = middle[:1]
     pl.semaphore_wait(barrier, devices - 1)
 
-    edge = halo_before.shape[1]
     halo_copies = [
         pltpu.make_async_remote_copy(
-            src_ref=streams_hbm.at[:, pl.ds(positions - edge, edge)],
-            dst_ref=halo_before,
-            send_sem=halo_sems.at[0],
-            recv_sem=halo_sems.at[1],
-            device_id=place(partner(1)),
+            src_ref=edges.at[side],
+            dst_ref=halo,
+            send_sem=halo_sems.at[2 * side],
+            recv_sem=halo_sems.at[2 * side + 1],
+            device_id=place(partner(step)),
             device_id_type=mesh_id,
-        ),
-        pltpu.make_async_remote_copy(
-            src_ref=streams_hbm.at[:, pl.ds(0, edge)],
-            dst_ref=halo_after,
-            send_sem=halo_sems.at[2],
-            recv_sem=halo_sems.at[3],
-            device_id=place(partner(devices - 1)),
-            device_id_type=mesh_id,
-        ),
+        )
+        for side, halo, step in ((0, halo_before, 1), (1, halo_after, devices - 1))
     ]
     for copy in halo_copies:
         copy.start()
@@ -353,15 +358,15 @@
 
     taps_copies = exchange(0, lambda device: taps_send.at[:, device], taps_recv.at[:, me])
 
-    loads[1].wait()
+    loads[2].wait()
     for copy in halo_copies:
         copy.wait()
     row = lax.broadcasted_iota(jnp.int32, (positions, channels), 0)
     smoothed = []
     for s in range(3):
         middle = streams[s].astype(jnp.float32)
-        before = jnp.where(me > 0, halo_before[s].astype(jnp.float32)[edge - 1 : edge], 0.0)
-        after = jnp.where(me < devices - 1, halo_after[s].astype(jnp.float32)[:1], 0.0)
+        before = jnp.where(me > 0, halo_before[s : s + 1], 0.0)
+        after = jnp.where(me < devices - 1, halo_after[s : s + 1], 0.0)
         previous = jnp.where(row == 0, before, pltpu.roll(middle, 1, 0))
         following = jnp.where(row == positions - 1, after, pltpu.roll(middle, positions - 1, 0))
         smoothed.append(
@@ -372,6 +377,8 @@
     gated_recv[me] = gated_send[me]
     gated_copies = exchange(1, lambda device: gated_send.at[device], gated_recv.at[me])
 
+    for load in loads[3:9]:
+        load.wait()
     groups = devices + 1
     rows = groups * share
     shape = (groups, share, positions)
@@ -395,8 +402,6 @@
         both = inner_product(jnp.concatenate([turned_real, turned_imag], axis=1), ((1,), (0,)))
         return both[:, :positions], both[:, positions:]
 
-    loads[2].wait()
-    loads[3].wait()
     for copy in taps_copies:
         copy.wait_recv()
     halves = jnp.concatenate(
@@ -435,9 +440,9 @@
     convolved = jnp.transpose(back_recv[...].reshape(channels, positions).astype(jnp.float32))
     mixed = ((convolved + gain_ref[...] * gated) * smoothed[0]).astype(jnp.bfloat16)
     mean_square = jnp.mean(jnp.square(mixed.astype(jnp.float32)), axis=-1, keepdims=True)
-    row_scale = lax.rsqrt(mean_square + EPSILON)
-    loads[4].wait()
-    out_ref[...] = (dot32(mixed, weight[...]) * row_scale).astype(jnp.bfloat16)
+    mixed_ref[...] = mixed
+    loads[9].wait()
+    scale_ref[...] = lax.rsqrt(mean_square + EPSILON)
     for copy in taps_copies + gated_copies + back_copies:
         copy.wait_send()
 
@@ -449,43 +454,74 @@
     share = channels // devices
     tables = host_tables(devices, share, positions)
     half = (devices, share, positions)
-    edge = 16
     anywhere = pl.BlockSpec(memory_space=pl.ANY)
     vector = pl.BlockSpec(memory_space=pltpu.VMEM)
-    outer_shape = tables[0].shape
-    projected = pl.pallas_call(
+    operands = (
+        streams.reshape(3, positions, channels),
+        filter_taps,
+        short_taps,
+        skip_gain.reshape(1, channels),
+        *(jnp.asarray(table) for table in tables),
+        out_weight,
+    )
+
+    def held(operand):
+        return pltpu.VMEM(operand.shape, operand.dtype)
+
+    mixed, row_scale, resident = pl.pallas_call(
         functools.partial(whole_kernel, axes, (devices, share, positions, channels)),
-        out_shape=jax.ShapeDtypeStruct((positions, width), jnp.bfloat16),
-        in_specs=[anywhere, anywhere, vector, vector, anywhere, anywhere, anywhere, vector, vector, vector],
-        out_specs=vector,
+        out_shape=[
+            pltpu.VMEM((positions, channels), jnp.bfloat16),
+            pltpu.VMEM((positions, 1), jnp.float32),
+            held(out_weight),
+        ],
+        in_specs=[anywhere] * len(operands),
+        out_specs=[vector, vector, vector],
         scratch_shapes=[
-            pltpu.VMEM((3, positions, channels), jnp.bfloat16),
-            pltpu.VMEM((2, positions, channels), jnp.float32),
-            pltpu.VMEM((channels, width), jnp.bfloat16),
-            pltpu.VMEM(outer_shape, jnp.bfloat16),
-            pltpu.VMEM(outer_shape, jnp.bfloat16),
-            pltpu.VMEM((3, edge, channels), jnp.bfloat16),
-            pltpu.VMEM((3, edge, channels), jnp.bfloat16),
+            *(held(operand) for operand in operands[:-1]),
+            pltpu.VMEM((2, 8, channels), jnp.float32),
+            pltpu.VMEM((8, channels), jnp.float32),
+            pltpu.VMEM((8, channels), jnp.float32),
             pltpu.VMEM((2, *half), jnp.bfloat16),
             pltpu.VMEM((2, *half), jnp.bfloat16),
             pltpu.VMEM(half, jnp.bfloat16),
             pltpu.VMEM(half, jnp.bfloat16),
             pltpu.VMEM(half, jnp.bfloat16),
             pltpu.VMEM(half, jnp.bfloat16),
-            pltpu.SemaphoreType.DMA((5,)),
+            pltpu.SemaphoreType.DMA((len(operands),)),
             pltpu.SemaphoreType.DMA((4,)),
             pltpu.SemaphoreType.DMA((3, devices)),
             pltpu.SemaphoreType.DMA((3, devices)),
         ],
-        compiler_params=pltpu.CompilerParams(collective_id=0, has_side_effects=True),
-    )(
-        streams.reshape(3, positions, channels),
-        filter_taps,
-        short_taps,
-        skip_gain.reshape(1, channels),
-        out_weight,
-        *(jnp.asarray(table) for table in tables),
-    )
+        compiler_params=pltpu.CompilerParams(
+            collective_id=0, has_side_effects=True, vmem_limit_bytes=24 * 2**20
+        ),
+        cost_estimate=pl.CostEstimate(flops=10**10, bytes_accessed=10**7, transcendentals=0),
+    )(*(pltpu.with_memory_space_constraint(operand, pltpu.HBM) for operand in operands))
+    chunks = 8
+    chunk = width // chunks
+
+    def project(mixed_ref, scale_ref, weight_ref, out_hbm, out_tiles, sems):
+        for i in range(chunks):
+            columns = pl.ds(i * chunk, chunk)
+            value = dot32(mixed_ref[...], weight_ref[:, columns]) * scale_ref[...]
+            out_tiles[:, columns] = value.astype(jnp.bfloat16)
+            pltpu.make_async_copy(out_tiles.at[:, columns], out_hbm.at[:, columns], sems.at[i]).start()
+        for i in range(chunks):
+            columns = pl.ds(i * chunk, chunk)
+            pltpu.make_async_copy(out_tiles.at[:, columns], out_hbm.at[:, columns], sems.at[i]).wait()
+
+    projected = pl.pallas_call(
+        project,
+        out_shape=jax.ShapeDtypeStruct((positions, width), jnp.bfloat16),
+        in_specs=[vector] * 3,
+        out_specs=anywhere,
+        scratch_shapes=[
+            pltpu.VMEM((positions, width), jnp.bfloat16),
+            pltpu.SemaphoreType.DMA((chunks,)),
+        ],
+        compiler_params=pltpu.CompilerParams(vmem_limit_bytes=16 * 2**20),
+    )(*(pltpu.with_memory_space_constraint(held_value, pltpu.VMEM) for held_value in (mixed, row_scale, resident)))
     return projected.reshape(1, positions, width)
 
 

time: 35.4 us -> 30.3 us (0.86)
  Pallas kernels: 32.9 us -> 30.1 us
  local copies, waits for them, and re-layouts: 2.29 us -> 0 us
    pallas_call x1, Pallas kernels: 32.9 us -> 28.7 us  [exchanged_once(): pl.pallas_call(functools.partial(whole_kernel, axes, (devices, share, pos...]
    unnamed x1 -> x0, local copies, waits for them, and re-layouts: 2.29 us -> none
    pallas_call x0 -> x1, Pallas kernels: none -> 1.46 us  [exchanged_once(): pl.pallas_call(project, out_shape=jax.ShapeDtypeStruct((positions, width)...]
where the time goes in v2:
time: 30.3 us; the launch traced here: 30.1 us
  Pallas kernels  30.1 us (99%)
    pallas_call x1, Pallas kernels, exchanged_once(): pl.pallas_call(functools.partial(whole_kernel, axes, (devices, share, pos...  28.7 us
    pallas_call x1, Pallas kernels, exchanged_once(): pl.pallas_call(project, out_shape=jax.ShapeDtypeStruct((positions, width)...  1.46 us

profile of v2, /device:TPU:0, one launch (start us, length us, event | category | flops | bytes accessed | tf_op | source)
XLA Modules:
  0.0 30.1 jit_solution(10804609550540261017)
XLA Ops:
  0.0 28.7 %shard_map.100 = (bf16[128,512]{1,0:T(8,128)(2,1)S(1)}, f32[128,1]{1,0:T(8,128)S(1)}, bf16[512,4096]{1,0:T(8,128)(2,1)S(1)}) custom-call(bf16[3,128,512]{2,1,0:T(8,128)(2,1)} %bitcast.3, f32[2,128,512]{2,1,0:T(8,128)} %taps_hbm.1, f32[3,3,512]{2,1,0:T(4,128)} %short_hbm.1, f32[1,512]{1,0:T(1,128)} %bitcast.4, ...), custom_call_target="tpu_custom_call" | custom-call | flops 10000000000 | bytes 10000000 | tf_op jit(solution)/shard_map/pallas_call | solution.py:471
  28.7 1.5 %shard_map.101 = bf16[128,4096]{1,0:T(8,128)(2,1)} custom-call(bf16[128,512]{1,0:T(8,128)(2,1)S(1)} %get-tuple-element.8.mixed_ref, f32[128,1]{1,0:T(8,128)S(1)} %get-tuple-element.9.scale_ref, bf16[512,4096]{1,0:T(8,128)(2,1)S(1)} %get-tuple-element.10.weight_ref), custom_call_target="tpu_custom_call" | custom-call | tf_op jit(solution)/shard_map/pallas_call | solution.py:514

commit v3 on v2

--- a/solution.py
+++ b/solution.py
@@ -272,7 +272,7 @@
     axes, sizes, streams_hbm, taps_hbm, short_hbm, gain_hbm, outer_high_hbm, outer_low_hbm,
     inner_high_hbm, inner_low_hbm, twiddle_hbm, weight_hbm, mixed_ref, scale_ref, weight_ref,
     streams, taps, short_ref, gain_ref, outer_high, outer_low, inner_high_ref, inner_low_ref, twiddle_ref,
-    edges, halo_before, halo_after,
+    turned_high, turned_low, edges, halo_before, halo_after,
     taps_send, taps_recv, gated_send, gated_recv, back_send, back_recv,
     local_sems, halo_sems, send_sems, recv_sems,
 ):
@@ -315,8 +315,8 @@
     loads[0].wait()
     for half in range(2):
         turned = jnp.transpose(taps[half]).astype(jnp.bfloat16)
-        taps_send[half] = turned.reshape(devices, share, positions)
-    taps_recv[:, me] = taps_send[:, me]
+        taps_send[:, half] = turned.reshape(devices, share, positions)
+    taps_recv[me] = taps_send[me]
     loads[1].wait()
     for s in range(3):
         middle = streams[s].astype(jnp.float32)
@@ -356,7 +356,7 @@
             copy.start()
         return copies
 
-    taps_copies = exchange(0, lambda device: taps_send.at[:, device], taps_recv.at[:, me])
+    taps_copies = exchange(0, lambda device: taps_send.at[device], taps_recv.at[me])
 
     loads[2].wait()
     for copy in halo_copies:
@@ -379,6 +379,8 @@
 
     for load in loads[3:9]:
         load.wait()
+    turned_high[...] = jnp.transpose(outer_high[...])
+    turned_low[...] = jnp.transpose(outer_low[...])
     groups = devices + 1
     rows = groups * share
     shape = (groups, share, positions)
@@ -405,7 +407,7 @@
     for copy in taps_copies:
         copy.wait_recv()
     halves = jnp.concatenate(
-        [taps_recv[half].reshape(devices * share, positions) for half in range(2)], axis=1
+        [taps_recv[:, half].reshape(devices * share, positions) for half in range(2)], axis=1
     )
     halves = outer_product(halves)
     part_row = lax.broadcasted_iota(jnp.int32, (2 * devices * share, positions), 0) // share
@@ -416,7 +418,7 @@
 
     for copy in gated_copies:
         copy.wait_recv()
-    signal_real, signal_imag = spectrum(outer_product(gated_recv[...].reshape(devices * share, positions)))
+    signal_real, signal_imag = spectrum(dot32(outer_high[...], gated_recv[...].reshape(devices * share, positions)))
     product_real, product_imag = complex_times(signal_real, signal_imag, kernel_real, kernel_imag)
     both = inner_product(jnp.concatenate([product_real, product_imag], axis=1), ((1,), (1,)))
     real_part, imag_part = both[:, :positions], both[:, positions:]
@@ -428,10 +430,8 @@
     back_imag = back_imag * (2.0 * scale)
     back = jnp.concatenate([back_real, back_imag[share : rows - share]], axis=0)
     high, low = split_pair(back)
-    dims = ((0,), (0,))
-    spatial = dot32(outer_high[...], high, dims) + (
-        dot32(outer_high[...], low, dims) + dot32(outer_low[...], high, dims)
-    )
+    both = dot32(turned_high[...], jnp.concatenate([high, low], axis=1))
+    spatial = both[:, :positions] + (both[:, positions:] + dot32(turned_low[...], high))
     back_send[...] = spatial.astype(jnp.bfloat16).reshape(devices, share, positions)
     back_recv[me] = back_send[me]
     back_copies = exchange(2, lambda device: back_send.at[device], back_recv.at[me])
@@ -479,11 +479,13 @@
         out_specs=[vector, vector, vector],
         scratch_shapes=[
             *(held(operand) for operand in operands[:-1]),
+            pltpu.VMEM(tables[0].shape[::-1], jnp.bfloat16),
+            pltpu.VMEM(tables[0].shape[::-1], jnp.bfloat16),
             pltpu.VMEM((2, 8, channels), jnp.float32),
             pltpu.VMEM((8, channels), jnp.float32),
             pltpu.VMEM((8, channels), jnp.float32),
-            pltpu.VMEM((2, *half), jnp.bfloat16),
-            pltpu.VMEM((2, *half), jnp.bfloat16),
+            pltpu.VMEM((devices, 2, share, positions), jnp.bfloat16),
+            pltpu.VMEM((devices, 2, share, positions), jnp.bfloat16),
             pltpu.VMEM(half, jnp.bfloat16),
             pltpu.VMEM(half, jnp.bfloat16),
             pltpu.VMEM(half, jnp.bfloat16),

time: 30.3 us -> 29.2 us (0.964)
  Pallas kernels: 30.1 us -> 29 us
    pallas_call x1, Pallas kernels: 28.7 us -> 27.5 us  [exchanged_once(): pl.pallas_call(functools.partial(whole_kernel, axes, (devices, share, pos...]
where the time goes in v3:
time: 29.2 us; the launch traced here: 29 us
  Pallas kernels  29 us (99%)
    pallas_call x1, Pallas kernels, exchanged_once(): pl.pallas_call(functools.partial(whole_kernel, axes, (devices, share, pos...  27.5 us
    pallas_call x1, Pallas kernels, exchanged_once(): pl.pallas_call(project, out_shape=jax.ShapeDtypeStruct((positions, width)...  1.46 us

profile of v3, /device:TPU:0, one launch (start us, length us, event | category | flops | bytes accessed | tf_op | source)
XLA Modules:
  0.0 29.0 jit_solution(14643935396006989946)
XLA Ops:
  0.0 27.5 %shard_map.100 = (bf16[128,512]{1,0:T(8,128)(2,1)S(1)}, f32[128,1]{1,0:T(8,128)S(1)}, bf16[512,4096]{1,0:T(8,128)(2,1)S(1)}) custom-call(bf16[3,128,512]{2,1,0:T(8,128)(2,1)} %bitcast.3, f32[2,128,512]{2,1,0:T(8,128)} %taps_hbm.1, f32[3,3,512]{2,1,0:T(4,128)} %short_hbm.1, f32[1,512]{1,0:T(1,128)} %bitcast.4, ...), custom_call_target="tpu_custom_call" | custom-call | flops 10000000000 | bytes 10000000 | tf_op jit(solution)/shard_map/pallas_call | solution.py:471
  27.6 1.5 %shard_map.101 = bf16[128,4096]{1,0:T(8,128)(2,1)} custom-call(bf16[128,512]{1,0:T(8,128)(2,1)S(1)} %get-tuple-element.8.mixed_ref, f32[128,1]{1,0:T(8,128)S(1)} %get-tuple-element.9.scale_ref, bf16[512,4096]{1,0:T(8,128)(2,1)S(1)} %get-tuple-element.10.weight_ref), custom_call_target="tpu_custom_call" | custom-call | tf_op jit(solution)/shard_map/pallas_call | solution.py:516
